TPU v7x, 32 devices: a whole 2x2x4 slice. The times are simulated.
32 devices in a mesh: fs: 4 (over y, x), tp: 8 (over z, core).
Axes of the slice: x: 2, y: 2, z: 4, core: 2. Of those that a mesh axis runs over, the one named last changes fastest.
Arguments:
- inputs: bfloat16 [1536, 2048], P('fs'), may hold values from -6 to 6
- pre_act: bfloat16 [1536, 8192], P('fs', 'tp'), may hold values from -6 to 6
- cotangent: bfloat16 [1536, 2048], P('fs'), may hold values from -6 to 6
- up_weight: bfloat16 [2048, 8192], P('fs', 'tp'), may hold values from -0.125 to 0.125
- down_weight: bfloat16 [8192, 2048], P('tp', 'fs'), may hold values from -0.0625 to 0.0625
Outputs:
- input_grad: bfloat16 [1536, 2048], P('fs')
- up_grad: float32 [2048, 8192], P('fs', 'tp')
- down_grad: float32 [8192, 2048], P('tp', 'fs')
- up_norms: float32 [2048], P('fs')
- down_norms: float32 [8192], P('tp')
All inputs are finite; a program needn't handle non-finite values.
Results may differ from a plain program's by a relative error of at most 0.0051.
Values may be sent and summed in bfloat16 or wider, within the bound.
A program may use at most 64 MiB of HBM per device.

v0:
```python
import jax
import jax.numpy as jnp
from jax import lax
from jax.sharding import PartitionSpec as P


def contract_last(left, right):
    return lax.dot_general(
        left, right, (((1,), (1,)), ((), ())), preferred_element_type=jnp.float32
    )


def contract_first(left, right):
    return lax.dot_general(
        left, right, (((0,), (0,)), ((), ())), preferred_element_type=jnp.float32
    )


def local(inputs, pre_act, cotangent, up_weight, down_weight):
    active = jnp.maximum(pre_act.astype(jnp.float32), 0.0)
    squared = (active * active).astype(jnp.bfloat16)
    sq_grad = contract_last(cotangent, lax.all_gather(down_weight, "fs", axis=1, tiled=True))
    pre_grad = (2.0 * active * sq_grad).astype(jnp.bfloat16)
    partial_value = contract_last(pre_grad, lax.all_gather(up_weight, "fs", axis=0, tiled=True))
    input_grad = lax.psum(partial_value, "tp").astype(jnp.bfloat16)
    input_cols, cotan_cols = (
        lax.all_to_all(inputs, "fs", split_axis=1, concat_axis=0, tiled=True),
        lax.all_to_all(cotangent, "fs", split_axis=1, concat_axis=0, tiled=True),
    )
    all_pre_grad, all_squared = (
        lax.all_gather(pre_grad, "fs", axis=0, tiled=True),
        lax.all_gather(squared, "fs", axis=0, tiled=True),
    )
    up_grad = contract_first(input_cols, all_pre_grad)
    down_grad = contract_first(all_squared, cotan_cols)
    up_norms = lax.psum(jnp.sum(up_grad * up_grad, axis=1), "tp")
    down_norms = lax.psum(jnp.sum(down_grad * down_grad, axis=1), "fs")
    return (input_grad, up_grad, down_grad, up_norms, down_norms)


def solution(mesh):
    in_specs = (P("fs", None), P("fs", "tp"), P("fs", None), P("fs", "tp"), P("tp", "fs"))
    out_specs = (P("fs", None), P("fs", "tp"), P("tp", "fs"), P("fs"), P("tp"))
    return jax.shard_map(local, mesh=mesh, in_specs=in_specs, out_specs=out_specs, check_vma=False)
```

profile of v0, /device:TPU:0, one launch (start us, length us, event | category | flops | bytes accessed | tf_op | source)
XLA Modules:
  0.0 329.2 jit_solution(1895293256298894493)
XLA Ops:
  7.2 0.0 copy-start.2
  7.2 0.0 all-gather.5.cloned.1.call-start
  7.2 0.7 all-gather.5.cloned.1.call-update
  7.9 0.0 copy-start.1
  7.9 0.0 all-gather.11.cloned.1.call-start
  8.0 0.3 copy-done.2
  8.3 1.1 multiply_convert_fusion
  9.4 0.0 all-gather.11.cloned.1.call-update
  9.4 0.0 all-gather.7.cloned.1.call-start
  9.5 0.7 all-gather.7.cloned.1.call-update
  10.1 0.0 all-gather.9.cloned.1.call-start
  10.2 54.8 %all-gather.5.cloned.1.call-done = bf16[1024,2048]{1,0:T(8,128)(2,1)} async-done(((bf16[1024,512]{1,0:T(8,128)(2,1)}), bf16[1024,2048]{1,0:T(8,128)(2,1)}) %all-gather.5.cloned.1.call-update) | async-done | bytes 4194320 | tf_op jit(solution)/shard_map/all_gather | solution.py:22
  65.0 0.0 copy-done.1
  65.0 0.0 copy-start
  65.0 5.2 %multiply_convert_fusion.1 = bf16[384,1024]{1,0:T(8,128)(2,1)} fusion(bf16[384,1024]{1,0:T(8,128)(2,1)} %param.6, bf16[384,2048]{1,0:T(8,128)(2,1)S(1)} %copy-done.1, bf16[1024,2048]{1,0:T(8,128)(2,1)} %all-gather.5.cloned.1.call-done), kind=kOutput, calls=%fused_computation.4 | convolution fusion | flops 1612578816 | bytes 7340032 | tf_op jit(solution)/shard_map/dot_general | solution.py:8
  70.2 0.0 all-gather.9.cloned.1.call-update
  70.3 0.0 copy-done
  70.3 1.6 copy.14
  71.8 3.6 %all-to-all-start = ((bf16[384,4,512]{0,2,1:T(8,128)(2,1)}), bf16[384,4,512]{0,2,1:T(8,128)(2,1)S(1)}, u32[]{:S(2)}, u32[]{:S(2)}) async-start(bf16[384,4,512]{0,2,1:T(8,128)(2,1)} %bitcast), calls=%async_computation | async-start | bytes 3145728 | tf_op jit(solution)/shard_map/all_to_all | solution.py:27
  75.5 1.6 copy.16
  77.0 25.8 %all-to-all-done = bf16[384,4,512]{0,2,1:T(8,128)(2,1)S(1)} async-done(((bf16[384,4,512]{0,2,1:T(8,128)(2,1)}), bf16[384,4,512]{0,2,1:T(8,128)(2,1)S(1)}, u32[]{:S(2)}, u32[]{:S(2)}) %all-to-all-start) | async-done | bytes 1572896 | tf_op jit(solution)/shard_map/all_to_all | solution.py:27
  102.9 3.6 %all-to-all-start.1 = ((bf16[384,4,512]{0,2,1:T(8,128)(2,1)}), bf16[384,4,512]{0,2,1:T(8,128)(2,1)S(1)}, u32[]{:S(2)}, u32[]{:S(2)}) async-start(bf16[384,4,512]{0,2,1:T(8,128)(2,1)} %bitcast.4), calls=%async_computation.1 | async-start | bytes 3145728 | tf_op jit(solution)/shard_map/all_to_all | solution.py:28
  106.4 1.6 copy.15
  108.1 34.6 %all-to-all-done.1 = bf16[384,4,512]{0,2,1:T(8,128)(2,1)S(1)} async-done(((bf16[384,4,512]{0,2,1:T(8,128)(2,1)}), bf16[384,4,512]{0,2,1:T(8,128)(2,1)S(1)}, u32[]{:S(2)}, u32[]{:S(2)}) %all-to-all-start.1) | async-done | bytes 1572896 | tf_op jit(solution)/shard_map/all_to_all | solution.py:28
  142.7 1.6 copy.17
  144.3 0.0 all-gather.11.cloned.1.call-done
  144.3 4.2 %multiply_reduce_fusion = (f32[1024]{0:T(1024)S(1)}, f32[1024,512]{0,1:T(8,128)S(1)}) fusion(bf16[1536,1024]{1,0:T(8,128)(2,1)} %all-gather.11.cloned.1.call-done, bf16[1536,512]{1,0:T(8,128)(2,1)} %bitcast.19), kind=kOutput, calls=%fused_computation | convolution fusion | flops 1611660288 | bytes 6819840 | tf_op jit(solution)/shard_map/dot_general | solution.py:14
  148.5 1.8 copy.19
  150.3 9.8 %psum.23 = f32[1024]{0:T(1024)} all-reduce(f32[1024]{0:T(1024)S(1)} %get-tuple-element.24), channel_id=1, replica_groups=mesh['fs'=4,'tp'=8] {'fs'}, use_global_device_ids=true, to_apply=%region_4.0 | all-reduce | flops 1024 | bytes 8192 | tf_op jit(solution)/shard_map/psum | solution.py:37
  160.1 37.4 %all-gather.7.cloned.1.call-done = bf16[2048,1024]{1,0:T(8,128)(2,1)} async-done(((bf16[512,1024]{1,0:T(8,128)(2,1)}), bf16[2048,1024]{1,0:T(8,128)(2,1)}) %all-gather.7.cloned.1.call-update) | async-done | bytes 4194320 | tf_op jit(solution)/shard_map/all_gather | solution.py:24
  197.5 4.3 %fusion = f32[384,2048]{1,0:T(8,128)S(1)} fusion(bf16[384,1024]{1,0:T(8,128)(2,1)} %multiply_convert_fusion.1, bf16[2048,1024]{1,0:T(8,128)(2,1)} %all-gather.7.cloned.1.call-done), kind=kOutput, calls=%fused_computation.6 | convolution fusion | flops 1610612736 | bytes 8126464 | tf_op jit(solution)/shard_map/dot_general | solution.py:8
  201.7 41.9 %all-gather.9.cloned.1.call-done = bf16[1536,1024]{1,0:T(8,128)(2,1)} async-done(((bf16[384,1024]{1,0:T(8,128)(2,1)}), bf16[1536,1024]{1,0:T(8,128)(2,1)}) %all-gather.9.cloned.1.call-update) | async-done | bytes 3145744 | tf_op jit(solution)/shard_map/all_gather | solution.py:31
  243.6 5.5 %multiply_reduce_fusion.1 = (f32[512]{0:T(512)S(1)}, f32[512,1024]{0,1:T(8,128)}) fusion(bf16[1536,1024]{1,0:T(8,128)(2,1)} %all-gather.9.cloned.1.call-done, bf16[1536,512]{1,0:T(8,128)(2,1)} %bitcast.18), kind=kOutput, calls=%fused_computation.1 | convolution fusion | flops 1611660800 | bytes 6817792 | tf_op jit(solution)/shard_map/dot_general | solution.py:14
  249.1 2.9 copy.18
  252.0 70.7 %all-reduce.2 = (bf16[384,2048]{1,0:T(8,128)(2,1)}, f32[512]{0:T(512)}) all-reduce(f32[384,2048]{1,0:T(8,128)S(1)} %fusion, f32[512]{0:T(512)S(1)} %get-tuple-element.22), channel_id=1, replica_groups=mesh['fs'=4,'tp'=8] {'tp'}, use_global_device_ids=true, to_apply=%region_0.0 | all-reduce | flops 786944 | bytes 4722688 | tf_op jit(solution)/shard_map/psum | solution.py:25
Async XLA Ops:
  7.2 1.1 copy-start.2
  7.2 57.8 %all-gather.5.cloned.1.call-start = ((), (), s32[]{:S(2)}) async-start(), calls=%async_computation.2 | async-start | bytes 5242880 | tf_op jit(solution)/shard_map/all_gather | solution.py:22
  7.9 57.1 %copy-start.1 = (bf16[384,2048]{1,0:T(8,128)(2,1)S(1)}, bf16[384,2048]{1,0:T(8,128)(2,1)}, u32[]{:S(2)}) copy-start(bf16[384,2048]{1,0:T(8,128)(2,1)} %param.7) | copy-start | bytes 4718596
  7.9 136.4 %all-gather.11.cloned.1.call-start = ((), (), s32[]{:S(2)}) async-start(), calls=%async_computation.5 | async-start | bytes 3932160 | tf_op jit(solution)/shard_map/all_gather | solution.py:32
  9.4 188.1 %all-gather.7.cloned.1.call-start = ((), (), s32[]{:S(2)}) async-start(), calls=%async_computation.3 | async-start | bytes 5242880 | tf_op jit(solution)/shard_map/all_gather | solution.py:24
  10.1 233.5 %all-gather.9.cloned.1.call-start = ((), (), s32[]{:S(2)}) async-start(), calls=%async_computation.4 | async-start | bytes 3932160 | tf_op jit(solution)/shard_map/all_gather | solution.py:31
  65.0 5.3 %copy-start = (bf16[384,2048]{1,0:T(8,128)(2,1)S(1)}, bf16[384,2048]{1,0:T(8,128)(2,1)}, u32[]{:S(2)}) copy-start(bf16[384,2048]{1,0:T(8,128)(2,1)} %param.5) | copy-start | bytes 4718596
  71.8 31.0 %all-to-all-start = ((bf16[384,4,512]{0,2,1:T(8,128)(2,1)}), bf16[384,4,512]{0,2,1:T(8,128)(2,1)S(1)}, u32[]{:S(2)}, u32[]{:S(2)}) async-start(bf16[384,4,512]{0,2,1:T(8,128)(2,1)} %bitcast), calls=%async_computation | async-start | bytes 3145728 | tf_op jit(solution)/shard_map/all_to_all | solution.py:27
  102.9 39.8 %all-to-all-start.1 = ((bf16[384,4,512]{0,2,1:T(8,128)(2,1)}), bf16[384,4,512]{0,2,1:T(8,128)(2,1)S(1)}, u32[]{:S(2)}, u32[]{:S(2)}) async-start(bf16[384,4,512]{0,2,1:T(8,128)(2,1)} %bitcast.4), calls=%async_computation.1 | async-start | bytes 3145728 | tf_op jit(solution)/shard_map/all_to_all | solution.py:28
Sparse Core Ops, SparseCore 0:
  9.8 55.1 all-gather.4
  66.8 76.1 all-gather.10
  144.8 52.5 all-gather.6
  199.8 43.8 all-gather.8
where the time goes:
time: 330 us; the launch traced here: 329 us
  waiting for transfers between devices  196 us (59%)
  blocking collectives  80.5 us (24%)
  matrix products  19.2 us (6%)
  between operations  13.8 us (4%)
  local copies, waits for them, and re-layouts  11.4 us (3%)
  starting transfers between devices  7.33 us (2%)
    psum x1, blocking collectives, local(): input_grad = lax.psum(partial_value, 'tp').astype(jnp.bfloat16)  70.7 us
    all_gather x1, waiting for transfers between devices, local(): lax.all_gather(down_weight, 'fs', axis=1, tiled=True)  54.8 us
    all_gather x1, waiting for transfers between devices, local(): lax.all_gather(pre_grad, 'fs', axis=0, tiled=True)  41.9 us
    all_gather x1, waiting for transfers between devices, local(): lax.all_gather(up_weight, 'fs', axis=0, tiled=True)  37.4 us
    all_to_all x1, waiting for transfers between devices, local(): lax.all_to_all(cotangent, 'fs', split_axis=1, concat_axis=0, tiled=True)  34.6 us
    all_to_all x1, waiting for transfers between devices, local(): lax.all_to_all(inputs, 'fs', split_axis=1, concat_axis=0, tiled=True)  25.8 us
    psum x1, blocking collectives, local(): down_norms = lax.psum(jnp.sum(down_grad * down_grad, axis=1), 'fs')  9.78 us
    dot_general x2, matrix products, contract_first(): lax.dot_general(left, right, (((0,), (0,)), ((), ())), preferred_element_...  9.7 us
  transfers between devices with their start and end apart: 6, of which 5 were waited for; matrix products, arithmetic and copies ran while one was open for 7% of the time, Pallas kernels for 0%

commit v1 on v0

--- a/solution.py
+++ b/solution.py
@@ -2,6 +2,27 @@
 import jax.numpy as jnp
 from jax import lax
 from jax.sharding import PartitionSpec as P
+
+
+def joined_along(parts, dim):
+    shape = list(parts.shape[1:])
+    shape[dim] *= parts.shape[0]
+    return jnp.moveaxis(parts, 0, dim).reshape(shape)
+
+
+def collected_by_bits(x, axis):
+    size, index = (lax.axis_size(axis), lax.axis_index(axis))
+    blocks, apart = (x[None], 1)
+    while apart < size:
+        other = lax.ppermute(blocks, axis, [(i, i ^ apart) for i in range(size)])
+        low = index & apart == 0
+        blocks = jnp.concatenate([jnp.where(low, blocks, other), jnp.where(low, other, blocks)])
+        apart *= 2
+    return blocks
+
+
+def gather_by_bits(shard, axis, dim):
+    return joined_along(collected_by_bits(shard, axis), dim)
 
 
 def contract_last(left, right):
@@ -21,7 +42,7 @@
     squared = (active * active).astype(jnp.bfloat16)
     sq_grad = contract_last(cotangent, lax.all_gather(down_weight, "fs", axis=1, tiled=True))
     pre_grad = (2.0 * active * sq_grad).astype(jnp.bfloat16)
-    partial_value = contract_last(pre_grad, lax.all_gather(up_weight, "fs", axis=0, tiled=True))
+    partial_value = contract_last(pre_grad, gather_by_bits(up_weight, "fs", 0))
     input_grad = lax.psum(partial_value, "tp").astype(jnp.bfloat16)
     input_cols, cotan_cols = (
         lax.all_to_all(inputs, "fs", split_axis=1, concat_axis=0, tiled=True),

time: 330 us -> 315 us (0.955)
  waiting for transfers between devices: 196 us -> 165 us
  other arithmetic: 1.08 us -> 9.31 us
  starting transfers between devices: 7.33 us -> 14 us
    all_to_all x1, waiting for transfers between devices: 34.6 us -> 81.7 us  [local(): lax.all_to_all(cotangent, 'fs', split_axis=1, concat_axis=0, tiled=True)]
    all_gather x1, waiting for transfers between devices: 41.9 us -> 0.02 us  [local(): lax.all_gather(pre_grad, 'fs', axis=0, tiled=True)]
    all_gather x1 -> x0, waiting for transfers between devices: 37.4 us -> none  [local(): lax.all_gather(up_weight, 'fs', axis=0, tiled=True)]
    all_gather x1, waiting for transfers between devices: 54.8 us -> 62.5 us  [local(): lax.all_gather(down_weight, 'fs', axis=1, tiled=True)]
    all_to_all x1, waiting for transfers between devices: 25.8 us -> 19.7 us  [local(): lax.all_to_all(inputs, 'fs', split_axis=1, concat_axis=0, tiled=True)]
    ppermute x0 -> x2, starting transfers between devices: none -> 4.99 us  [collected_by_bits(): other = lax.ppermute(blocks, axis, [(i, i ^ apart) for i in range(size)])]
    concatenate x0 -> x2, other arithmetic: none -> 3.86 us  [collected_by_bits(): jnp.concatenate([jnp.where(low, blocks, other), jnp.where(low, other, blo...]
  transfers between devices with their start and end apart: 6 -> 7, of which waited for: 5 -> 3; matrix products, arithmetic and copies ran while one was open for 7% -> 11% of each run, Pallas kernels for 0% -> 0%
where the time goes in v1:
time: 315 us
  waiting for transfers between devices  165 us (52%)
  blocking collectives  79.9 us (25%)
  matrix products  19.1 us (6%)
  local copies, waits for them, and re-layouts  14 us (4%)
  starting transfers between devices  14 us (4%)
  between operations  13.9 us (4%)
  other arithmetic  9.31 us (3%)
    all_to_all x1, waiting for transfers between devices, local(): lax.all_to_all(cotangent, 'fs', split_axis=1, concat_axis=0, tiled=True)  81.7 us
    psum x1, blocking collectives, local(): input_grad = lax.psum(partial_value, 'tp').astype(jnp.bfloat16)  70.4 us
    all_gather x1, waiting for transfers between devices, local(): lax.all_gather(down_weight, 'fs', axis=1, tiled=True)  62.5 us
    all_to_all x1, waiting for transfers between devices, local(): lax.all_to_all(inputs, 'fs', split_axis=1, concat_axis=0, tiled=True)  19.7 us
    dot_general x2, matrix products, contract_first(): lax.dot_general(left, right, (((0,), (0,)), ((), ())), preferred_element_...  9.71 us
    psum x1, blocking collectives, local(): down_norms = lax.psum(jnp.sum(down_grad * down_grad, axis=1), 'fs')  9.55 us
    dot_general x2, matrix products, contract_last(): lax.dot_general(left, right, (((1,), (1,)), ((), ())), preferred_element_...  9.39 us
    unnamed x10, local copies, waits for them, and re-layouts  8.86 us
  transfers between devices with their start and end apart: 7, of which 3 were waited for; matrix products, arithmetic and copies ran while one was open for 11% of the time, Pallas kernels for 0%

profile of v1, /device:TPU:0, one launch (start us, length us, event | category | flops | bytes accessed | tf_op | source)
XLA Modules:
  0.0 314.8 jit_solution(9926232925607691505)
XLA Ops:
  7.2 0.0 copy-start.1
  7.2 0.0 all-gather.4.cloned.1.call-start
  7.2 0.7 all-gather.4.cloned.1.call-update
  7.9 0.0 all-gather.8.cloned.1.call-start
  8.0 2.2 multiply_convert_fusion
  10.2 0.0 all-gather.8.cloned.1.call-update
  10.2 0.0 all-gather.6.cloned.1.call-start
  10.2 0.0 copy-start
  10.3 3.0 collective-permute-start
  13.3 62.5 %all-gather.4.cloned.1.call-done = bf16[1024,2048]{1,0:T(8,128)(2,1)} async-done(((bf16[1024,512]{1,0:T(8,128)(2,1)}), bf16[1024,2048]{1,0:T(8,128)(2,1)}) %all-gather.4.cloned.1.call-update) | async-done | bytes 4194320 | tf_op jit(solution)/shard_map/all_gather | solution.py:43
  75.8 0.0 copy-done.1
  75.8 5.1 %multiply_convert_fusion.1 = bf16[384,1024]{1,0:T(8,128)(2,1)} fusion(bf16[384,1024]{1,0:T(8,128)(2,1)} %param.6, bf16[384,2048]{1,0:T(8,128)(2,1)S(1)} %copy-done.1, bf16[1024,2048]{1,0:T(8,128)(2,1)} %all-gather.4.cloned.1.call-done), kind=kOutput, calls=%fused_computation.8 | convolution fusion | flops 1612578816 | bytes 7340032 | tf_op jit(solution)/shard_map/dot_general | solution.py:29
  81.0 0.0 all-gather.6.cloned.1.call-update
  81.0 0.0 copy-done
  81.0 1.6 copy.14
  82.6 0.0 copy-start.2
  82.6 4.5 %all-to-all-start = ((bf16[384,4,512]{0,2,1:T(8,128)(2,1)}), bf16[384,4,512]{0,2,1:T(8,128)(2,1)}, u32[]{:S(2)}, u32[]{:S(2)}) async-start(bf16[384,4,512]{0,2,1:T(8,128)(2,1)} %bitcast.2), calls=%async_computation | async-start | bytes 3145728 | tf_op jit(solution)/shard_map/all_to_all | solution.py:48
  87.1 0.0 collective-permute-done
  87.1 0.0 copy-done.2
  87.1 1.4 broadcast_select_fusion.3
  88.5 1.5 pad_maximum_fusion.1
  90.0 2.0 collective-permute-start.1
  92.0 2.6 copy.16
  94.5 19.7 %all-to-all-done = bf16[384,4,512]{0,2,1:T(8,128)(2,1)} async-done(((bf16[384,4,512]{0,2,1:T(8,128)(2,1)}), bf16[384,4,512]{0,2,1:T(8,128)(2,1)}, u32[]{:S(2)}, u32[]{:S(2)}) %all-to-all-start) | async-done | bytes 1572896 | tf_op jit(solution)/shard_map/all_to_all | solution.py:48
  114.2 4.3 %all-to-all-start.1 = ((bf16[384,4,512]{0,2,1:T(8,128)(2,1)}), bf16[384,4,512]{0,2,1:T(8,128)(2,1)}, u32[]{:S(2)}, u32[]{:S(2)}) async-start(bf16[384,4,512]{0,2,1:T(8,128)(2,1)} %bitcast.20), calls=%async_computation.1 | async-start | bytes 3145728 | tf_op jit(solution)/shard_map/all_to_all | solution.py:49
  118.6 2.6 copy.15
  121.1 81.7 %all-to-all-done.1 = bf16[384,4,512]{0,2,1:T(8,128)(2,1)} async-done(((bf16[384,4,512]{0,2,1:T(8,128)(2,1)}), bf16[384,4,512]{0,2,1:T(8,128)(2,1)}, u32[]{:S(2)}, u32[]{:S(2)}) %all-to-all-start.1) | async-done | bytes 1572896 | tf_op jit(solution)/shard_map/all_to_all | solution.py:49
  202.8 2.6 copy.17
  205.4 0.0 collective-permute-done.1
  205.4 1.9 broadcast_select_fusion.1
  207.3 2.4 pad_maximum_fusion
  209.6 0.0 all-gather.8.cloned.1.call-done
  209.6 4.2 %multiply_reduce_fusion = (f32[1024]{0:T(1024)S(1)}, f32[1024,512]{0,1:T(8,128)S(1)}) fusion(bf16[1536,1024]{1,0:T(8,128)(2,1)} %all-gather.8.cloned.1.call-done, bf16[1536,512]{1,0:T(8,128)(2,1)} %bitcast.23), kind=kOutput, calls=%fused_computation.2 | convolution fusion | flops 1611660288 | bytes 6819840 | tf_op jit(solution)/shard_map/dot_general | solution.py:35
  213.8 1.8 copy.19
  215.6 9.6 %psum.23 = f32[1024]{0:T(1024)} all-reduce(f32[1024]{0:T(1024)S(1)} %get-tuple-element.28), channel_id=1, replica_groups=mesh['fs'=4,'tp'=8] {'fs'}, use_global_device_ids=true, to_apply=%region_4.5 | all-reduce | flops 1024 | bytes 8192 | tf_op jit(solution)/shard_map/psum | solution.py:58
  225.2 4.3 %fusion = f32[384,2048]{1,0:T(8,128)S(1)} fusion(bf16[384,1024]{1,0:T(8,128)(2,1)} %multiply_convert_fusion.1, bf16[2048,1024]{1,0:T(8,128)(2,1)} %bitcast.21), kind=kOutput, calls=%fused_computation.12 | convolution fusion | flops 1610612736 | bytes 8126464 | tf_op jit(solution)/shard_map/dot_general | solution.py:29
  229.4 0.0 all-gather.6.cloned.1.call-done
  229.5 5.5 %multiply_reduce_fusion.1 = (f32[512]{0:T(512)S(1)}, f32[512,1024]{0,1:T(8,128)}) fusion(bf16[1536,1024]{1,0:T(8,128)(2,1)} %all-gather.6.cloned.1.call-done, bf16[1536,512]{1,0:T(8,128)(2,1)} %bitcast.22), kind=kOutput, calls=%fused_computation.3 | convolution fusion | flops 1611660800 | bytes 6817792 | tf_op jit(solution)/shard_map/dot_general | solution.py:35
  235.0 2.9 copy.18
  237.9 70.4 %all-reduce.2 = (bf16[384,2048]{1,0:T(8,128)(2,1)}, f32[512]{0:T(512)}) all-reduce(f32[384,2048]{1,0:T(8,128)S(1)} %fusion, f32[512]{0:T(512)S(1)} %get-tuple-element.26), channel_id=1, replica_groups=mesh['fs'=4,'tp'=8] {'tp'}, use_global_device_ids=true, to_apply=%region_0.1 | all-reduce | flops 786944 | bytes 4722688 | tf_op jit(solution)/shard_map/psum | solution.py:46
Async XLA Ops:
  7.2 68.7 %copy-start.1 = (bf16[384,2048]{1,0:T(8,128)(2,1)S(1)}, bf16[384,2048]{1,0:T(8,128)(2,1)}, u32[]{:S(2)}) copy-start(bf16[384,2048]{1,0:T(8,128)(2,1)} %param.7) | copy-start | bytes 4718596
  7.2 68.7 %all-gather.4.cloned.1.call-start = ((), (), s32[]{:S(2)}) async-start(), calls=%async_computation.2 | async-start | bytes 5242880 | tf_op jit(solution)/shard_map/all_gather | solution.py:43
  7.9 201.7 %all-gather.8.cloned.1.call-start = ((), (), s32[]{:S(2)}) async-start(), calls=%async_computation.4 | async-start | bytes 3932160 | tf_op jit(solution)/shard_map/all_gather | solution.py:53
  10.2 219.3 %all-gather.6.cloned.1.call-start = ((), (), s32[]{:S(2)}) async-start(), calls=%async_computation.3 | async-start | bytes 3932160 | tf_op jit(solution)/shard_map/all_gather | solution.py:52
  10.2 70.8 %copy-start = (bf16[384,2048]{1,0:T(8,128)(2,1)S(1)}, bf16[384,2048]{1,0:T(8,128)(2,1)}, u32[]{:S(2)}) copy-start(bf16[384,2048]{1,0:T(8,128)(2,1)} %param.5) | copy-start | bytes 4718596
  10.3 76.9 %collective-permute-start = (bf16[1,512,1024]{2,1,0:T(8,128)(2,1)}, bf16[1,512,1024]{2,1,0:T(8,128)(2,1)}, u32[]{:S(2)}, u32[]{:S(2)}) collective-permute-start(bf16[1,512,1024]{2,1,0:T(8,128)(2,1)} %bitcast.24), channel_id=1, source_target_pairs={{0,8},{8,0},{16,24},{24,16},{1,9},{9,1},{17,25},{25,17},{2,10},{10... | collective-permute-start | bytes 3145736 | tf_op jit(solution)/shard_map/ppermute | solution.py:17
  82.6 4.6 %copy-start.2 = (bf16[512,1024]{1,0:T(8,128)(2,1)S(1)}, bf16[512,1024]{1,0:T(8,128)(2,1)}, u32[]{:S(2)}) copy-start(bf16[512,1024]{1,0:T(8,128)(2,1)} %param.8) | copy-start | bytes 3145732
  82.6 31.6 %all-to-all-start = ((bf16[384,4,512]{0,2,1:T(8,128)(2,1)}), bf16[384,4,512]{0,2,1:T(8,128)(2,1)}, u32[]{:S(2)}, u32[]{:S(2)}) async-start(bf16[384,4,512]{0,2,1:T(8,128)(2,1)} %bitcast.2), calls=%async_computation | async-start | bytes 3145728 | tf_op jit(solution)/shard_map/all_to_all | solution.py:48
  90.0 115.4 %collective-permute-start.1 = (bf16[2,512,1024]{2,1,0:T(8,128)(2,1)}, bf16[2,512,1024]{2,1,0:T(8,128)(2,1)}, u32[]{:S(2)}, u32[]{:S(2)}) collective-permute-start(bf16[2,512,1024]{2,1,0:T(8,128)(2,1)} %pad_maximum_fusion.1), channel_id=1, source_target_pairs={{0,16},{8,24},{16,0},{24,8},{1,17},{9,25},{17,1},{25,9},{2,18},{10... | collective-permute-start | bytes 6291464 | tf_op jit(solution)/shard_map/ppermute | solution.py:17
  114.2 88.6 %all-to-all-start.1 = ((bf16[384,4,512]{0,2,1:T(8,128)(2,1)}), bf16[384,4,512]{0,2,1:T(8,128)(2,1)}, u32[]{:S(2)}, u32[]{:S(2)}) async-start(bf16[384,4,512]{0,2,1:T(8,128)(2,1)} %bitcast.20), calls=%async_computation.1 | async-start | bytes 3145728 | tf_op jit(solution)/shard_map/all_to_all | solution.py:49
Sparse Core Ops, SparseCore 0:
  9.8 65.9 all-gather.3
  77.7 84.3 all-gather.7
  163.9 53.9 all-gather.5
